TPU v7x, 32 devices: a whole 2x2x4 slice. The times are simulated.
32 devices in a mesh: grp: 2 (over x), sp: 4 (over y, core), tp: 4 (over z).
Axes of the slice: x: 2, y: 2, z: 4, core: 2. Of those that a mesh axis runs over, the one named last changes fastest.
Arguments:
- tokens_in: bfloat16 [2048, 2048], P(('grp', 'sp'), 'tp'), parts along dimension 0, may hold values from -8 to 8
- out_gate: bfloat16 [3, 2048, 2048], P(None, 'sp', 'tp'), may hold values from -0.125 to 0.125
- in_gate: bfloat16 [3, 2048, 2048], P(None, 'sp', 'tp'), may hold values from -0.125 to 0.125
- value_proj: bfloat16 [3, 2048, 2048], P(None, 'sp', 'tp'), may hold values from -0.125 to 0.125
- mix_proj: bfloat16 [3, 2048, 2048], P(None, 'sp', 'tp'), may hold values from -0.125 to 0.125
- conv_taps: float32 [3, 3, 2048], P(None, None, 'tp'), may hold values from -3.5 to 3.5
- norm_gains: float32 [3, 2048], P(None, 'tp'), may hold values from 0.1 to 1.9
- final_gain: float32 [2048], P('tp'), may hold values from 0.1 to 1.9
Outputs:
- normed_out: bfloat16 [2048, 2048], P(('grp', 'sp'), 'tp'), parts along dimension 0
There are 2 independent parts, one for each index of `grp`. A program takes and returns all parts, laid end to end along the dimension named above; an argument that names none is the same for every part. Nothing has to cross between parts.
All inputs are finite; a program needn't handle non-finite values.
Results may differ from a plain program's by a relative error of at most 0.025.
Values may be sent and summed in bfloat16 or wider, within the bound.
A program may use at most 64 MiB of HBM per device.

v0:
```python
import jax
import jax.numpy as jnp
from jax import lax
from jax.sharding import PartitionSpec as P

D = 2048
TAPS = 3
LAYERS = 3
epsilon = 1e-06


def passed_along(shard, axis, by):
    peers = lax.axis_size(axis)
    pairs = [(i, i + by) for i in range(peers) if 0 <= i + by < peers]
    return lax.ppermute(shard, axis, pairs)


def row_scale(stream):
    squares = lax.psum(jnp.sum(stream * stream, axis=1, keepdims=True), "tp")
    return lax.rsqrt(squares / D + epsilon)


def shards(tokens_in, out_gate, in_gate, value_proj, mix_proj, conv_taps, norm_gains, final_gain):
    stream = tokens_in.astype(jnp.float32)
    row_count = stream.shape[0]
    reach = TAPS - 1
    whole = (
        lax.all_gather(out_gate, "sp", axis=1, tiled=True),
        lax.all_gather(in_gate, "sp", axis=1, tiled=True),
        lax.all_gather(value_proj, "sp", axis=1, tiled=True),
        lax.all_gather(mix_proj, "sp", axis=1, tiled=True),
    )
    for layer_index in range(LAYERS):
        scale = row_scale(stream)
        normed = (stream * norm_gains[layer_index]).astype(jnp.bfloat16)
        gathered = lax.all_gather(normed, "tp", axis=1, tiled=True)
        products = tuple(
            (
                jnp.dot(gathered, weight[layer_index], preferred_element_type=jnp.float32)
                for weight in whole[:3]
            )
        )
        out_gates, in_gates, values = [
            (product * scale).astype(jnp.bfloat16) for product in products
        ]
        product_v = (in_gates.astype(jnp.float32) * values.astype(jnp.float32)).astype(jnp.bfloat16)
        earlier = passed_along(product_v[row_count - reach :], "sp", 1)
        padded = jnp.concatenate([earlier, product_v], axis=0)
        convolved = padded[0:row_count].astype(jnp.float32) * conv_taps[layer_index, 0]
        for tap_index in range(1, TAPS):
            convolved = (
                convolved
                + padded[tap_index : tap_index + row_count].astype(jnp.float32)
                * conv_taps[layer_index, tap_index]
            )
        gated = (out_gates.astype(jnp.float32) * convolved).astype(jnp.bfloat16)
        spread = lax.all_gather(gated, "tp", axis=1, tiled=True)
        mixed = jnp.dot(spread, whole[3][layer_index], preferred_element_type=jnp.float32)
        stream = stream + mixed
    scale = row_scale(stream)
    return (stream * scale * final_gain).astype(jnp.bfloat16)


def solution(mesh):
    in_specs = (
        P(("grp", "sp"), "tp"),
        P(None, "sp", "tp"),
        P(None, "sp", "tp"),
        P(None, "sp", "tp"),
        P(None, "sp", "tp"),
        P(None, None, "tp"),
        P(None, "tp"),
        P("tp"),
    )
    out_specs = P(("grp", "sp"), "tp")
    return jax.shard_map(shards, mesh=mesh, in_specs=in_specs, out_specs=out_specs, check_vma=False)
```

profile of v0, /device:TPU:0, one launch (start us, length us, event | category | flops | bytes accessed | tf_op | source)
XLA Modules:
  0.0 424.5 jit_solution(9574232206159354128)
XLA Ops:
  6.5 0.8 fusion.60
  7.4 1.7 fusion.55
  11.8 13.5 %psum.28 = f32[256,1]{0,1:T(1,128)S(1)} all-reduce(f32[256,1]{0,1:T(1,128)S(1)} %bitcast.159), channel_id=1, replica_groups=mesh['grp'=2,'sp'=4,'tp'=4] {'tp'}, use_global_device_ids=true, to_apply=%region_1.0 | all-reduce | flops 256 | bytes 2048 | tf_op jit(solution)/shard_map/psum | solution.py:19
  25.3 14.7 %all-gather.11.cloned.1.call-done = bf16[256,2048]{1,0:T(8,128)(2,1)} async-done(((bf16[256,512]{1,0:T(8,128)(2,1)}), bf16[256,2048]{1,0:T(8,128)(2,1)}) %all-gather.11.cloned.1.call-update) | async-done | bytes 1048592 | tf_op jit(solution)/shard_map/all_gather | solution.py:36
  40.0 47.3 %all-gather.17.cloned.1.call-done = bf16[3,2048,512]{2,1,0:T(8,128)(2,1)} async-done(((bf16[3,512,512]{2,1,0:T(8,128)(2,1)}), bf16[3,2048,512]{2,1,0:T(8,128)(2,1)}) %all-gather.17.cloned.1.call-update) | async-done | bytes 6291472 | tf_op jit(solution)/shard_map/all_gather | solution.py:30
  87.3 2.6 fusion.39
  90.0 45.3 %all-gather.15.cloned.1.call-done = bf16[3,2048,512]{2,1,0:T(8,128)(2,1)} async-done(((bf16[3,512,512]{2,1,0:T(8,128)(2,1)}), bf16[3,2048,512]{2,1,0:T(8,128)(2,1)}) %all-gather.15.cloned.1.call-update) | async-done | bytes 6291472 | tf_op jit(solution)/shard_map/all_gather | solution.py:29
  135.3 2.6 fusion.38
  137.9 2.2 collective-permute-start
  140.1 43.0 %all-gather.13.cloned.1.call-done = bf16[3,2048,512]{2,1,0:T(8,128)(2,1)} async-done(((bf16[3,512,512]{2,1,0:T(8,128)(2,1)}), bf16[3,2048,512]{2,1,0:T(8,128)(2,1)}) %all-gather.13.cloned.1.call-update) | async-done | bytes 6291472 | tf_op jit(solution)/shard_map/all_gather | solution.py:28
  183.1 3.1 fusion.35
  186.3 44.6 %all-gather.21.cloned.1.call-done = bf16[3,2048,512]{2,1,0:T(8,128)(2,1)} async-done(((bf16[3,512,512]{2,1,0:T(8,128)(2,1)}), bf16[3,2048,512]{2,1,0:T(8,128)(2,1)}) %all-gather.21.cloned.1.call-update) | async-done | bytes 6291472 | tf_op jit(solution)/shard_map/all_gather | solution.py:31
  230.9 29.4 %all-gather.19.cloned.1.call-done = bf16[256,2048]{1,0:T(8,128)(2,1)} async-done(((bf16[256,512]{1,0:T(8,128)(2,1)}), bf16[256,2048]{1,0:T(8,128)(2,1)}) %all-gather.19.cloned.1.call-update) | async-done | bytes 1048592 | tf_op jit(solution)/shard_map/all_gather | solution.py:57
  260.3 3.4 multiply_reduce_fusion.2
  263.8 10.3 %psum.29 = f32[256,1]{0,1:T(1,128)S(1)} all-reduce(f32[256,1]{0,1:T(1,128)S(1)} %bitcast.182), channel_id=1, replica_groups=mesh['grp'=2,'sp'=4,'tp'=4] {'tp'}, use_global_device_ids=true, to_apply=%region_3.0 | all-reduce | flops 256 | bytes 2048 | tf_op jit(solution)/shard_map/psum | solution.py:19
  274.1 17.2 %all-gather.23.cloned.1.call-done = bf16[256,2048]{1,0:T(8,128)(2,1)} async-done(((bf16[256,512]{1,0:T(8,128)(2,1)}), bf16[256,2048]{1,0:T(8,128)(2,1)}) %all-gather.23.cloned.1.call-update) | async-done | bytes 1048592 | tf_op jit(solution)/shard_map/all_gather | solution.py:36
  291.2 2.7 fusion.46
  293.9 2.6 fusion.45
  296.6 1.3 collective-permute-start.1
  298.7 3.1 fusion.42
  301.9 30.3 %all-gather.25.cloned.1.call-done = bf16[256,2048]{1,0:T(8,128)(2,1)} async-done(((bf16[256,512]{1,0:T(8,128)(2,1)}), bf16[256,2048]{1,0:T(8,128)(2,1)}) %all-gather.25.cloned.1.call-update) | async-done | bytes 1048592 | tf_op jit(solution)/shard_map/all_gather | solution.py:57
  332.2 3.3 multiply_reduce_fusion.1
  335.6 10.3 %psum.30 = f32[256,1]{0,1:T(1,128)S(1)} all-reduce(f32[256,1]{0,1:T(1,128)S(1)} %bitcast.181), channel_id=1, replica_groups=mesh['grp'=2,'sp'=4,'tp'=4] {'tp'}, use_global_device_ids=true, to_apply=%region_5.0 | all-reduce | flops 256 | bytes 2048 | tf_op jit(solution)/shard_map/psum | solution.py:19
  345.9 17.2 %all-gather.27.cloned.1.call-done = bf16[256,2048]{1,0:T(8,128)(2,1)} async-done(((bf16[256,512]{1,0:T(8,128)(2,1)}), bf16[256,2048]{1,0:T(8,128)(2,1)}) %all-gather.27.cloned.1.call-update) | async-done | bytes 1048592 | tf_op jit(solution)/shard_map/all_gather | solution.py:36
  363.0 2.7 fusion.53
  365.7 2.6 fusion.52
  368.4 1.3 collective-permute-start.2
  370.5 3.1 fusion.49
  373.6 30.3 %all-gather.29.cloned.1.call-done = bf16[256,2048]{1,0:T(8,128)(2,1)} async-done(((bf16[256,512]{1,0:T(8,128)(2,1)}), bf16[256,2048]{1,0:T(8,128)(2,1)}) %all-gather.29.cloned.1.call-update) | async-done | bytes 1048592 | tf_op jit(solution)/shard_map/all_gather | solution.py:57
  404.0 2.7 multiply_reduce_fusion
  406.7 10.2 %psum.31 = f32[256,1]{0,1:T(1,128)S(1)} all-reduce(f32[256,1]{0,1:T(1,128)S(1)} %bitcast.183), channel_id=1, replica_groups=mesh['grp'=2,'sp'=4,'tp'=4] {'tp'}, use_global_device_ids=true, to_apply=%region_7.0 | all-reduce | flops 256 | bytes 2048 | tf_op jit(solution)/shard_map/psum | solution.py:19
  416.8 0.8 multiply_convert_fusion
  (43 shorter events, 4.6 us)
Async XLA Ops:
  6.5 33.5 %all-gather.11.cloned.1.call-start = ((), (), s32[]{:S(2)}) async-start(), calls=%async_computation | async-start | bytes 1310720 | tf_op jit(solution)/shard_map/all_gather | solution.py:36
  9.1 78.2 %all-gather.17.cloned.1.call-start = ((), (), s32[]{:S(2)}) async-start(), calls=%async_computation.3 | async-start | bytes 7864320 | tf_op jit(solution)/shard_map/all_gather | solution.py:30
  9.9 125.4 %all-gather.15.cloned.1.call-start = ((), (), s32[]{:S(2)}) async-start(), calls=%async_computation.2 | async-start | bytes 7864320 | tf_op jit(solution)/shard_map/all_gather | solution.py:29
  10.6 129.5 %copy-start.1 = (f32[3,3,512]{2,1,0:T(4,128)S(1)}, f32[3,3,512]{2,1,0:T(4,128)}, u32[]{:S(2)}) copy-start(f32[3,3,512]{2,1,0:T(4,128)} %param.13) | copy-start | bytes 55300
  10.6 172.5 %all-gather.13.cloned.1.call-start = ((), (), s32[]{:S(2)}) async-start(), calls=%async_computation.1 | async-start | bytes 7864320 | tf_op jit(solution)/shard_map/all_gather | solution.py:28
  11.2 219.7 %all-gather.21.cloned.1.call-start = ((), (), s32[]{:S(2)}) async-start(), calls=%async_computation.5 | async-start | bytes 7864320 | tf_op jit(solution)/shard_map/all_gather | solution.py:31
  11.8 248.6 %all-gather.19.cloned.1.call-start = ((), (), s32[]{:S(2)}) async-start(), calls=%async_computation.4 | async-start | bytes 1310720 | tf_op jit(solution)/shard_map/all_gather | solution.py:57
  40.0 143.1 %copy-start.3 = (bf16[256,2048]{1,0:T(8,128)(2,1)S(1)}, bf16[256,2048]{1,0:T(8,128)(2,1)}, u32[]{:S(2)}) copy-start(bf16[256,2048]{1,0:T(8,128)(2,1)} %all-gather.11.cloned.1.call-done) | copy-start | bytes 3145732
  90.0 170.4 %copy-start = (bf16[256,512]{1,0:T(8,128)(2,1)S(1)}, bf16[256,512]{1,0:T(8,128)(2,1)}, u32[]{:S(2)}) copy-start(bf16[256,512]{1,0:T(8,128)(2,1)} %param.8) | copy-start | bytes 786436
  137.9 45.2 %collective-permute-start = (bf16[2,512]{1,0:T(2,128)(2,1)S(1)}, bf16[2,512]{1,0:T(2,128)(2,1)S(1)}, u32[]{:S(2)}, u32[]{:S(2)}) collective-permute-start(bf16[2,512]{1,0:T(2,128)(2,1)S(1)} %slice.135), channel_id=1, source_target_pairs={{0,4},{4,8},{8,12},{1,5},{5,9},{9,13},{2,6},{6,10},{10,14},{3,7},{... | collective-permute-start | bytes 6152 | tf_op jit(solution)/shard_map/ppermute | solution.py:15
  186.2 105.0 %all-gather.23.cloned.1.call-start = ((), (), s32[]{:S(2)}) async-start(), calls=%async_computation.6 | async-start | bytes 1310720 | tf_op jit(solution)/shard_map/all_gather | solution.py:36
  263.7 68.4 %all-gather.25.cloned.1.call-start = ((), (), s32[]{:S(2)}) async-start(), calls=%async_computation.7 | async-start | bytes 1310720 | tf_op jit(solution)/shard_map/all_gather | solution.py:57
  291.2 7.5 %copy-start.5 = (bf16[256,2048]{1,0:T(8,128)(2,1)S(1)}, bf16[256,2048]{1,0:T(8,128)(2,1)}, u32[]{:S(2)}) copy-start(bf16[256,2048]{1,0:T(8,128)(2,1)} %all-gather.23.cloned.1.call-done) | copy-start | bytes 3145732
  296.6 2.1 collective-permute-start.1
  301.8 61.2 %all-gather.27.cloned.1.call-start = ((), (), s32[]{:S(2)}) async-start(), calls=%async_computation.8 | async-start | bytes 1310720 | tf_op jit(solution)/shard_map/all_gather | solution.py:36
  335.5 68.4 %all-gather.29.cloned.1.call-start = ((), (), s32[]{:S(2)}) async-start(), calls=%async_computation.9 | async-start | bytes 1310720 | tf_op jit(solution)/shard_map/all_gather | solution.py:57
  363.0 7.5 %copy-start.4 = (bf16[256,2048]{1,0:T(8,128)(2,1)S(1)}, bf16[256,2048]{1,0:T(8,128)(2,1)}, u32[]{:S(2)}) copy-start(bf16[256,2048]{1,0:T(8,128)(2,1)} %all-gather.27.cloned.1.call-done) | copy-start | bytes 3145732
  368.4 48.5 %copy-start.2 = (f32[512]{0:T(512)S(1)}, f32[512]{0:T(512)}, u32[]{:S(2)}) copy-start(f32[512]{0:T(512)} %param.15) | copy-start | bytes 6148
  368.4 2.1 collective-permute-start.2
Sparse Core Ops, SparseCore 0:
  9.2 30.7 all-gather.10
  41.6 45.7 all-gather.16
  88.9 46.3 all-gather.14
  136.7 46.3 all-gather.12
  184.5 46.3 all-gather.20
  232.3 27.9 all-gather.18
  263.8 27.3 all-gather.22
  302.0 30.1 all-gather.24
  335.6 27.3 all-gather.26
  373.8 30.1 all-gather.28
where the time goes:
time: 425 us
  waiting for transfers between devices  323 us (76%)
  blocking collectives  44.2 us (10%)
  matrix products  34.6 us (8%)
  between operations  13.7 us (3%)
  starting transfers between devices  5.1 us (1%)
    all_gather x3, waiting for transfers between devices, shards(): spread = lax.all_gather(gated, 'tp', axis=1, tiled=True)  90 us
    all_gather x3, waiting for transfers between devices, shards(): gathered = lax.all_gather(normed, 'tp', axis=1, tiled=True)  49.1 us
    all_gather x1, waiting for transfers between devices, shards(): lax.all_gather(value_proj, 'sp', axis=1, tiled=True)  47.3 us
    all_gather x1, waiting for transfers between devices, shards(): lax.all_gather(in_gate, 'sp', axis=1, tiled=True)  45.3 us
    all_gather x1, waiting for transfers between devices, shards(): lax.all_gather(mix_proj, 'sp', axis=1, tiled=True)  44.6 us
    psum x4, blocking collectives, row_scale(): squares = lax.psum(jnp.sum(stream * stream, axis=1, keepdims=True), 'tp')  44.2 us
    all_gather x1, waiting for transfers between devices, shards(): lax.all_gather(out_gate, 'sp', axis=1, tiled=True)  43 us
    dot_general x9, matrix products, shards(): jnp.dot(gathered, weight[layer_index], preferred_element_type=jnp.float32)  25.2 us
  transfers between devices with their start and end apart: 13, of which 12 were waited for; matrix products, arithmetic and copies ran while one was open for 2% of the time, Pallas kernels for 0%

commit v1 on v0

--- a/solution.py
+++ b/solution.py
@@ -54,7 +54,14 @@
                 * conv_taps[layer_index, tap_index]
             )
         gated = (out_gates.astype(jnp.float32) * convolved).astype(jnp.bfloat16)
-        spread = lax.all_gather(gated, "tp", axis=1, tiled=True)
+        ring = [gated]
+        for hop in range(3):
+            ring.append(lax.ppermute(ring[-1], "tp", [(dev, (dev + 1) % 4) for dev in range(4)]))
+        spread = jnp.roll(
+            jnp.concatenate(ring[::-1], axis=1),
+            (lax.axis_index("tp") + 1) * ring[0].shape[1],
+            axis=1,
+        )
         mixed = jnp.dot(spread, whole[3][layer_index], preferred_element_type=jnp.float32)
         stream = stream + mixed
     scale = row_scale(stream)

time: 425 us -> 393 us (0.925)
  waiting for transfers between devices: 323 us -> 291 us
  starting transfers between devices: 5.1 us -> 9.44 us
    all_gather x3 -> x0, waiting for transfers between devices: 90 us -> none  [shards(): spread = lax.all_gather(gated, 'tp', axis=1, tiled=True)]
    ppermute x0 -> x9, waiting for transfers between devices: none -> 77.1 us  [shards(): lax.ppermute(ring[-1], 'tp', [(dev, (dev + 1) % 4) for dev in range(4)])]
    all_gather x1, waiting for transfers between devices: 44.6 us -> 25.7 us  [shards(): lax.all_gather(mix_proj, 'sp', axis=1, tiled=True)]
    ppermute x0 -> x9, starting transfers between devices: none -> 4.44 us  [shards(): lax.ppermute(ring[-1], 'tp', [(dev, (dev + 1) % 4) for dev in range(4)])]
  transfers between devices with their start and end apart: 13 -> 19, of which waited for: 12 -> 17; matrix products, arithmetic and copies ran while one was open for 2% -> 2% of each run, Pallas kernels for 0% -> 0%
where the time goes in v1:
time: 393 us
  waiting for transfers between devices  291 us (74%)
  blocking collectives  42.3 us (11%)
  matrix products  33.3 us (8%)
  between operations  13.6 us (3%)
  starting transfers between devices  9.44 us (2%)
    ppermute x9, waiting for transfers between devices, shards(): lax.ppermute(ring[-1], 'tp', [(dev, (dev + 1) % 4) for dev in range(4)])  77.1 us
    all_gather x3, waiting for transfers between devices, shards(): gathered = lax.all_gather(normed, 'tp', axis=1, tiled=True)  47.8 us
    all_gather x1, waiting for transfers between devices, shards(): lax.all_gather(value_proj, 'sp', axis=1, tiled=True)  47.3 us
    all_gather x1, waiting for transfers between devices, shards(): lax.all_gather(in_gate, 'sp', axis=1, tiled=True)  45.2 us
    all_gather x1, waiting for transfers between devices, shards(): lax.all_gather(out_gate, 'sp', axis=1, tiled=True)  43.3 us
    psum x4, blocking collectives, row_scale(): squares = lax.psum(jnp.sum(stream * stream, axis=1, keepdims=True), 'tp')  42.3 us
    all_gather x1, waiting for transfers between devices, shards(): lax.all_gather(mix_proj, 'sp', axis=1, tiled=True)  25.7 us
    dot_general x9, matrix products, shards(): jnp.dot(gathered, weight[layer_index], preferred_element_type=jnp.float32)  22.3 us
  transfers between devices with their start and end apart: 19, of which 17 were waited for; matrix products, arithmetic and copies ran while one was open for 2% of the time, Pallas kernels for 0%

profile of v1, /device:TPU:0, one launch (start us, length us, event | category | flops | bytes accessed | tf_op | source)
XLA Modules:
  0.0 392.7 jit_solution(13088888377769784734)
XLA Ops:
  11.8 13.5 %psum.28 = f32[256,1]{0,1:T(1,128)S(1)} all-reduce(f32[256,1]{0,1:T(1,128)S(1)} %bitcast.156), channel_id=1, replica_groups=mesh['grp'=2,'sp'=4,'tp'=4] {'tp'}, use_global_device_ids=true, to_apply=%region_1.0 | all-reduce | flops 256 | bytes 2048 | tf_op jit(solution)/shard_map/psum | solution.py:19
  25.3 14.7 %all-gather.8.cloned.1.call-done = bf16[256,2048]{1,0:T(8,128)(2,1)} async-done(((bf16[256,512]{1,0:T(8,128)(2,1)}), bf16[256,2048]{1,0:T(8,128)(2,1)}) %all-gather.8.cloned.1.call-update) | async-done | bytes 1048592 | tf_op jit(solution)/shard_map/all_gather | solution.py:36
  40.0 47.3 %all-gather.14.cloned.1.call-done = bf16[3,2048,512]{2,1,0:T(8,128)(2,1)} async-done(((bf16[3,512,512]{2,1,0:T(8,128)(2,1)}), bf16[3,2048,512]{2,1,0:T(8,128)(2,1)}) %all-gather.14.cloned.1.call-update) | async-done | bytes 6291472 | tf_op jit(solution)/shard_map/all_gather | solution.py:30
  87.3 2.7 fusion.39
  90.1 45.2 %all-gather.12.cloned.1.call-done = bf16[3,2048,512]{2,1,0:T(8,128)(2,1)} async-done(((bf16[3,512,512]{2,1,0:T(8,128)(2,1)}), bf16[3,2048,512]{2,1,0:T(8,128)(2,1)}) %all-gather.12.cloned.1.call-update) | async-done | bytes 6291472 | tf_op jit(solution)/shard_map/all_gather | solution.py:29
  135.3 2.3 fusion.38
  137.6 2.2 collective-permute-start
  139.8 43.3 %all-gather.10.cloned.1.call-done = bf16[3,2048,512]{2,1,0:T(8,128)(2,1)} async-done(((bf16[3,512,512]{2,1,0:T(8,128)(2,1)}), bf16[3,2048,512]{2,1,0:T(8,128)(2,1)}) %all-gather.10.cloned.1.call-update) | async-done | bytes 6291472 | tf_op jit(solution)/shard_map/all_gather | solution.py:28
  183.1 2.4 fusion.35
  187.1 8.8 %collective-permute-done.1 = bf16[256,512]{1,0:T(8,128)(2,1)S(1)} collective-permute-done((bf16[256,512]{1,0:T(8,128)(2,1)S(1)}, bf16[256,512]{1,0:T(8,128)(2,1)S(1)}, u32[]{:S(2)}, u32[]{:S(2)}) %collective-permute-start.1) | collective-permute-done | bytes 262176 | tf_op jit(solution)/shard_map/ppermute | solution.py:59
  195.9 9.4 %collective-permute-done.2 = bf16[256,512]{1,0:T(8,128)(2,1)S(1)} collective-permute-done((bf16[256,512]{1,0:T(8,128)(2,1)S(1)}, bf16[256,512]{1,0:T(8,128)(2,1)S(1)}, u32[]{:S(2)}, u32[]{:S(2)}) %collective-permute-start.2) | collective-permute-done | bytes 262176 | tf_op jit(solution)/shard_map/ppermute | solution.py:59
  205.3 25.7 %all-gather.16.cloned.1.call-done = bf16[3,2048,512]{2,1,0:T(8,128)(2,1)} async-done(((bf16[3,512,512]{2,1,0:T(8,128)(2,1)}), bf16[3,2048,512]{2,1,0:T(8,128)(2,1)}) %all-gather.16.cloned.1.call-update) | async-done | bytes 6291472 | tf_op jit(solution)/shard_map/all_gather | solution.py:31
  230.9 3.9 multiply_reduce_fusion.2
  234.9 11.9 %psum.29 = f32[256,1]{0,1:T(1,128)S(1)} all-reduce(f32[256,1]{0,1:T(1,128)S(1)} %bitcast.178), channel_id=1, replica_groups=mesh['grp'=2,'sp'=4,'tp'=4] {'tp'}, use_global_device_ids=true, to_apply=%region_3.5 | all-reduce | flops 256 | bytes 2048 | tf_op jit(solution)/shard_map/psum | solution.py:19
  246.8 16.3 %all-gather.18.cloned.1.call-done = bf16[256,2048]{1,0:T(8,128)(2,1)} async-done(((bf16[256,512]{1,0:T(8,128)(2,1)}), bf16[256,2048]{1,0:T(8,128)(2,1)}) %all-gather.18.cloned.1.call-update) | async-done | bytes 1048592 | tf_op jit(solution)/shard_map/all_gather | solution.py:36
  263.1 2.7 fusion.46
  265.8 2.3 fusion.45
  270.2 2.4 fusion.42
  274.0 8.6 %collective-permute-done.5 = bf16[256,512]{1,0:T(8,128)(2,1)S(1)} collective-permute-done((bf16[256,512]{1,0:T(8,128)(2,1)S(1)}, bf16[256,512]{1,0:T(8,128)(2,1)S(1)}, u32[]{:S(2)}, u32[]{:S(2)}) %collective-permute-start.5) | collective-permute-done | bytes 262176 | tf_op jit(solution)/shard_map/ppermute | solution.py:59
  282.7 10.9 %collective-permute-done.6 = bf16[256,512]{1,0:T(8,128)(2,1)S(1)} collective-permute-done((bf16[256,512]{1,0:T(8,128)(2,1)S(1)}, bf16[256,512]{1,0:T(8,128)(2,1)S(1)}, u32[]{:S(2)}, u32[]{:S(2)}) %collective-permute-start.6) | collective-permute-done | bytes 262176 | tf_op jit(solution)/shard_map/ppermute | solution.py:59
  293.5 10.0 %collective-permute-done.7 = bf16[256,512]{1,0:T(8,128)(2,1)S(1)} collective-permute-done((bf16[256,512]{1,0:T(8,128)(2,1)S(1)}, bf16[256,512]{1,0:T(8,128)(2,1)S(1)}, u32[]{:S(2)}, u32[]{:S(2)}) %collective-permute-start.7) | collective-permute-done | bytes 262176 | tf_op jit(solution)/shard_map/ppermute | solution.py:59
  303.5 3.9 multiply_reduce_fusion.1
  307.4 8.5 %psum.30 = f32[256,1]{0,1:T(1,128)S(1)} all-reduce(f32[256,1]{0,1:T(1,128)S(1)} %bitcast.179), channel_id=1, replica_groups=mesh['grp'=2,'sp'=4,'tp'=4] {'tp'}, use_global_device_ids=true, to_apply=%region_5.7 | all-reduce | flops 256 | bytes 2048 | tf_op jit(solution)/shard_map/psum | solution.py:19
  315.9 16.9 %all-gather.20.cloned.1.call-done = bf16[256,2048]{1,0:T(8,128)(2,1)} async-done(((bf16[256,512]{1,0:T(8,128)(2,1)}), bf16[256,2048]{1,0:T(8,128)(2,1)}) %all-gather.20.cloned.1.call-update) | async-done | bytes 1048592 | tf_op jit(solution)/shard_map/all_gather | solution.py:36
  332.8 2.7 fusion.53
  335.5 2.3 fusion.52
  340.0 2.4 fusion.49
  343.9 8.4 %collective-permute-done.9 = bf16[256,512]{1,0:T(8,128)(2,1)S(1)} collective-permute-done((bf16[256,512]{1,0:T(8,128)(2,1)S(1)}, bf16[256,512]{1,0:T(8,128)(2,1)S(1)}, u32[]{:S(2)}, u32[]{:S(2)}) %collective-permute-start.9) | collective-permute-done | bytes 262176 | tf_op jit(solution)/shard_map/ppermute | solution.py:59
  352.3 11.0 %collective-permute-done.10 = bf16[256,512]{1,0:T(8,128)(2,1)S(1)} collective-permute-done((bf16[256,512]{1,0:T(8,128)(2,1)S(1)}, bf16[256,512]{1,0:T(8,128)(2,1)S(1)}, u32[]{:S(2)}, u32[]{:S(2)}) %collective-permute-start.10) | collective-permute-done | bytes 262176 | tf_op jit(solution)/shard_map/ppermute | solution.py:59
  363.2 10.1 %collective-permute-done.11 = bf16[256,512]{1,0:T(8,128)(2,1)S(1)} collective-permute-done((bf16[256,512]{1,0:T(8,128)(2,1)S(1)}, bf16[256,512]{1,0:T(8,128)(2,1)S(1)}, u32[]{:S(2)}, u32[]{:S(2)}) %collective-permute-start.11) | collective-permute-done | bytes 262176 | tf_op jit(solution)/shard_map/ppermute | solution.py:59
  373.4 3.3 multiply_reduce_fusion
  376.6 8.4 %psum.31 = f32[256,1]{0,1:T(1,128)S(1)} all-reduce(f32[256,1]{0,1:T(1,128)S(1)} %bitcast.180), channel_id=1, replica_groups=mesh['grp'=2,'sp'=4,'tp'=4] {'tp'}, use_global_device_ids=true, to_apply=%region_7.9 | all-reduce | flops 256 | bytes 2048 | tf_op jit(solution)/shard_map/psum | solution.py:19
  (52 shorter events, 14.8 us)
Async XLA Ops:
  6.5 33.5 %all-gather.8.cloned.1.call-start = ((), (), s32[]{:S(2)}) async-start(), calls=%async_computation | async-start | bytes 1310720 | tf_op jit(solution)/shard_map/all_gather | solution.py:36
  9.1 78.2 %all-gather.14.cloned.1.call-start = ((), (), s32[]{:S(2)}) async-start(), calls=%async_computation.3 | async-start | bytes 7864320 | tf_op jit(solution)/shard_map/all_gather | solution.py:30
  9.9 125.4 %all-gather.12.cloned.1.call-start = ((), (), s32[]{:S(2)}) async-start(), calls=%async_computation.2 | async-start | bytes 7864320 | tf_op jit(solution)/shard_map/all_gather | solution.py:29
  10.6 172.5 %all-gather.10.cloned.1.call-start = ((), (), s32[]{:S(2)}) async-start(), calls=%async_computation.1 | async-start | bytes 7864320 | tf_op jit(solution)/shard_map/all_gather | solution.py:28
  11.2 219.7 %all-gather.16.cloned.1.call-start = ((), (), s32[]{:S(2)}) async-start(), calls=%async_computation.4 | async-start | bytes 7864320 | tf_op jit(solution)/shard_map/all_gather | solution.py:31
  11.8 251.3 %all-gather.18.cloned.1.call-start = ((), (), s32[]{:S(2)}) async-start(), calls=%async_computation.5 | async-start | bytes 1310720 | tf_op jit(solution)/shard_map/all_gather | solution.py:36
  87.3 48.0 %copy-start.3 = (bf16[256,2048]{1,0:T(8,128)(2,1)S(1)}, bf16[256,2048]{1,0:T(8,128)(2,1)}, u32[]{:S(2)}) copy-start(bf16[256,2048]{1,0:T(8,128)(2,1)} %all-gather.8.cloned.1.call-done) | copy-start | bytes 3145732
  90.0 49.7 %copy-start.1 = (f32[3,3,512]{2,1,0:T(4,128)S(1)}, f32[3,3,512]{2,1,0:T(4,128)}, u32[]{:S(2)}) copy-start(f32[3,3,512]{2,1,0:T(4,128)} %param.15) | copy-start | bytes 55300
  137.6 45.5 %collective-permute-start = (bf16[2,512]{1,0:T(2,128)(2,1)S(1)}, bf16[2,512]{1,0:T(2,128)(2,1)S(1)}, u32[]{:S(2)}, u32[]{:S(2)}) collective-permute-start(bf16[2,512]{1,0:T(2,128)(2,1)S(1)} %slice.135), channel_id=1, source_target_pairs={{0,4},{4,8},{8,12},{1,5},{5,9},{9,13},{2,6},{6,10},{10,14},{3,7},{... | collective-permute-start | bytes 6152 | tf_op jit(solution)/shard_map/ppermute | solution.py:15
  183.1 47.8 %copy-start = (bf16[256,512]{1,0:T(8,128)(2,1)S(1)}, bf16[256,512]{1,0:T(8,128)(2,1)}, u32[]{:S(2)}) copy-start(bf16[256,512]{1,0:T(8,128)(2,1)} %param.10) | copy-start | bytes 786436
  185.5 10.3 %collective-permute-start.1 = (bf16[256,512]{1,0:T(8,128)(2,1)S(1)}, bf16[256,512]{1,0:T(8,128)(2,1)S(1)}, u32[]{:S(2)}, u32[]{:S(2)}) collective-permute-start(bf16[256,512]{1,0:T(8,128)(2,1)S(1)} %fusion.35), channel_id=1, source_target_pairs={{0,1},{1,2},{2,3},{3,0},{4,5},{5,6},{6,7},{7,4},{8,9},{9,10},{10,1... | collective-permute-start | bytes 786440 | tf_op jit(solution)/shard_map/ppermute | solution.py:59
  195.9 9.4 %collective-permute-start.2 = (bf16[256,512]{1,0:T(8,128)(2,1)S(1)}, bf16[256,512]{1,0:T(8,128)(2,1)S(1)}, u32[]{:S(2)}, u32[]{:S(2)}) collective-permute-start(bf16[256,512]{1,0:T(8,128)(2,1)S(1)} %collective-permute-done.1), channel_id=1, source_target_pairs={{0,1},{1,2},{2,3},{3,0},{4,5},{5,6},{6,7},{7,4},{8,9},{9,10},{10,1... | collective-permute-start | bytes 786440 | tf_op jit(solution)/shard_map/ppermute | solution.py:59
  205.3 25.7 %collective-permute-start.3 = (bf16[256,512]{1,0:T(8,128)(2,1)S(1)}, bf16[256,512]{1,0:T(8,128)(2,1)S(1)}, u32[]{:S(2)}, u32[]{:S(2)}) collective-permute-start(bf16[256,512]{1,0:T(8,128)(2,1)S(1)} %collective-permute-done.2), channel_id=1, source_target_pairs={{0,1},{1,2},{2,3},{3,0},{4,5},{5,6},{6,7},{7,4},{8,9},{9,10},{10,1... | collective-permute-start | bytes 786440 | tf_op jit(solution)/shard_map/ppermute | solution.py:59
  234.8 98.0 %all-gather.20.cloned.1.call-start = ((), (), s32[]{:S(2)}) async-start(), calls=%async_computation.6 | async-start | bytes 1310720 | tf_op jit(solution)/shard_map/all_gather | solution.py:36
  263.1 2.7 copy-start.5
  268.1 2.1 collective-permute-start.4
  272.7 10.0 %collective-permute-start.5 = (bf16[256,512]{1,0:T(8,128)(2,1)S(1)}, bf16[256,512]{1,0:T(8,128)(2,1)S(1)}, u32[]{:S(2)}, u32[]{:S(2)}) collective-permute-start(bf16[256,512]{1,0:T(8,128)(2,1)S(1)} %fusion.42), channel_id=1, source_target_pairs={{0,1},{1,2},{2,3},{3,0},{4,5},{5,6},{6,7},{7,4},{8,9},{9,10},{10,1... | collective-permute-start | bytes 786440 | tf_op jit(solution)/shard_map/ppermute | solution.py:59
  282.6 10.9 %collective-permute-start.6 = (bf16[256,512]{1,0:T(8,128)(2,1)S(1)}, bf16[256,512]{1,0:T(8,128)(2,1)S(1)}, u32[]{:S(2)}, u32[]{:S(2)}) collective-permute-start(bf16[256,512]{1,0:T(8,128)(2,1)S(1)} %collective-permute-done.5), channel_id=1, source_target_pairs={{0,1},{1,2},{2,3},{3,0},{4,5},{5,6},{6,7},{7,4},{8,9},{9,10},{10,1... | collective-permute-start | bytes 786440 | tf_op jit(solution)/shard_map/ppermute | solution.py:59
  293.5 10.0 %collective-permute-start.7 = (bf16[256,512]{1,0:T(8,128)(2,1)S(1)}, bf16[256,512]{1,0:T(8,128)(2,1)S(1)}, u32[]{:S(2)}, u32[]{:S(2)}) collective-permute-start(bf16[256,512]{1,0:T(8,128)(2,1)S(1)} %collective-permute-done.6), channel_id=1, source_target_pairs={{0,1},{1,2},{2,3},{3,0},{4,5},{5,6},{6,7},{7,4},{8,9},{9,10},{10,1... | collective-permute-start | bytes 786440 | tf_op jit(solution)/shard_map/ppermute | solution.py:59
  332.8 2.7 copy-start.4
  337.9 2.1 collective-permute-start.8
  342.4 9.9 %collective-permute-start.9 = (bf16[256,512]{1,0:T(8,128)(2,1)S(1)}, bf16[256,512]{1,0:T(8,128)(2,1)S(1)}, u32[]{:S(2)}, u32[]{:S(2)}) collective-permute-start(bf16[256,512]{1,0:T(8,128)(2,1)S(1)} %fusion.49), channel_id=1, source_target_pairs={{0,1},{1,2},{2,3},{3,0},{4,5},{5,6},{6,7},{7,4},{8,9},{9,10},{10,1... | collective-permute-start | bytes 786440 | tf_op jit(solution)/shard_map/ppermute | solution.py:59
  352.3 11.0 %collective-permute-start.10 = (bf16[256,512]{1,0:T(8,128)(2,1)S(1)}, bf16[256,512]{1,0:T(8,128)(2,1)S(1)}, u32[]{:S(2)}, u32[]{:S(2)}) collective-permute-start(bf16[256,512]{1,0:T(8,128)(2,1)S(1)} %collective-permute-done.9), channel_id=1, source_target_pairs={{0,1},{1,2},{2,3},{3,0},{4,5},{5,6},{6,7},{7,4},{8,9},{9,10},{10,1... | collective-permute-start | bytes 786440 | tf_op jit(solution)/shard_map/ppermute | solution.py:59
  363.2 10.1 %collective-permute-start.11 = (bf16[256,512]{1,0:T(8,128)(2,1)S(1)}, bf16[256,512]{1,0:T(8,128)(2,1)S(1)}, u32[]{:S(2)}, u32[]{:S(2)}) collective-permute-start(bf16[256,512]{1,0:T(8,128)(2,1)S(1)} %collective-permute-done.10), channel_id=1, source_target_pairs={{0,1},{1,2},{2,3},{3,0},{4,5},{5,6},{6,7},{7,4},{8,9},{9,10},{10,1... | collective-permute-start | bytes 786440 | tf_op jit(solution)/shard_map/ppermute | solution.py:59
  373.4 11.7 %copy-start.2 = (f32[512]{0:T(512)S(1)}, f32[512]{0:T(512)}, u32[]{:S(2)}) copy-start(f32[512]{0:T(512)} %param.17) | copy-start | bytes 6148
Sparse Core Ops, SparseCore 0:
  9.2 30.7 all-gather.7
  41.6 45.7 all-gather.13
  88.9 46.3 all-gather.11
  136.7 46.3 all-gather.9
  184.5 46.3 all-gather.15
  234.9 28.0 all-gather.17
  307.6 25.1 all-gather.19
